TPU v7x, 32 devices: a whole 2x2x4 slice. The times are simulated.
32 devices in a mesh: rep: 2 (over x), fs: 4 (over z), tp: 4 (over y, core).
Axes of the slice: x: 2, y: 2, z: 4, core: 2. Of those that a mesh axis runs over, the one named last changes fastest.
Arguments:
- tokens: bfloat16 [4096, 1024], P(('rep', 'fs', 'tp')), may hold values from -6 to 6
- w_up: bfloat16 [1024, 4096], P('fs', 'tp'), may hold values from -0.1875 to 0.1875
- w_down: bfloat16 [4096, 1024], P('tp', 'fs'), may hold values from -0.09375 to 0.09375
- out_gain: float32 [1024], replicated, may hold values from 0.1 to 1.9
- out_shift: float32 [1024], replicated, may hold values from -3 to 3
Outputs:
- normed: bfloat16 [4096, 1024], P(('rep', 'fs', 'tp'))
All inputs are finite; a program needn't handle non-finite values.
Results may differ from a plain program's by a relative error of at most 0.015.
Values may be sent and summed in bfloat16 or wider, within the bound.
A program may use at most 64 MiB of HBM per device.

v0:
```python
import jax
import jax.numpy as jnp
from jax import lax
from jax.sharding import PartitionSpec as P

residual_scale = 2.0**0.25
norm_eps = 1e-05


def over_all(share, axis, dim, apply):
    everything = lax.all_gather(share, axis, axis=dim, tiled=True)
    return apply(everything, jnp.int32(0))


def summed_rows(product, extent, axis):
    whole = product(jnp.int32(0), extent * lax.axis_size(axis)).astype(jnp.bfloat16)
    return lax.psum_scatter(whole, axis, scatter_dimension=0, tiled=True).astype(jnp.float32)


def layer_norm(summed, out_gain, out_shift):
    row_mean = jnp.mean(summed, axis=-1, keepdims=True)
    centered = summed - row_mean
    row_var = jnp.mean(centered * centered, axis=-1, keepdims=True)
    return centered * lax.rsqrt(row_var + norm_eps) * out_gain + out_shift


def squared_relu(pre_act):
    return jnp.square(jnp.maximum(pre_act, 0.0)).astype(jnp.bfloat16)


def shards(tokens, w_up, w_down, out_gain, out_shift):
    up_block = lax.all_gather(w_up, "fs", axis=0, tiled=True)

    def activate(block_rows, offset):
        return squared_relu(jnp.dot(block_rows, up_block, preferred_element_type=jnp.float32))

    hidden = over_all(tokens, "tp", 0, activate)
    down_block = lax.all_gather(w_down, "fs", axis=1, tiled=True)
    own_count = tokens.shape[0]

    def project(offset, how_many):
        picked = lax.dynamic_slice_in_dim(hidden, offset, how_many, 0)
        return jnp.dot(picked, down_block, preferred_element_type=jnp.float32)

    branch = summed_rows(project, own_count, "tp")
    summed = residual_scale * tokens.astype(jnp.float32) + branch
    return layer_norm(summed, out_gain, out_shift).astype(jnp.bfloat16)


def solution(mesh):
    in_specs = (P(("rep", "fs", "tp"), None), P("fs", "tp"), P("tp", "fs"), P(), P())
    out_specs = P(("rep", "fs", "tp"), None)
    return jax.shard_map(shards, mesh=mesh, in_specs=in_specs, out_specs=out_specs, check_vma=False)
```

profile of v0, /device:TPU:0, one launch (start us, length us, event | category | flops | bytes accessed | tf_op | source)
XLA Modules:
  0.0 162.0 jit_solution(3515093248988575749)
XLA Ops:
  6.5 0.0 all-gather.4.cloned.1.call-start
  6.5 0.7 all-gather.4.cloned.1.call-update
  7.3 0.0 all-gather.6.cloned.1.call-start
  7.3 0.7 all-gather.6.cloned.1.call-update
  8.0 0.0 all-gather.8.cloned.1.call-start
  8.1 0.7 all-gather.8.cloned.1.call-update
  8.7 0.0 copy-start
  8.8 0.0 reduce-scatter.2.cloned.1.call-start
  8.8 19.6 %all-gather.4.cloned.1.call-done = bf16[512,1024]{1,0:T(8,128)(2,1)} async-done(((bf16[128,1024]{1,0:T(8,128)(2,1)}), bf16[512,1024]{1,0:T(8,128)(2,1)}) %all-gather.4.cloned.1.call-update) | async-done | bytes 1048592 | tf_op jit(solution)/shard_map/all_gather | solution.py:11
  28.3 47.3 %all-gather.6.cloned.1.call-done = bf16[1024,1024]{1,0:T(8,128)(2,1)} async-done(((bf16[256,1024]{1,0:T(8,128)(2,1)}), bf16[1024,1024]{1,0:T(8,128)(2,1)}) %all-gather.6.cloned.1.call-update) | async-done | bytes 2097168 | tf_op jit(solution)/shard_map/all_gather | solution.py:32
  75.6 46.7 %all-gather.8.cloned.1.call-done = bf16[1024,1024]{1,0:T(8,128)(2,1)} async-done(((bf16[1024,256]{1,0:T(8,128)(2,1)}), bf16[1024,1024]{1,0:T(8,128)(2,1)}) %all-gather.8.cloned.1.call-update) | async-done | bytes 2097168 | tf_op jit(solution)/shard_map/all_gather | solution.py:38
  122.3 5.8 %convolution_convert_fusion = bf16[512,1024]{1,0:T(8,128)(2,1)} fusion(bf16[1024,1024]{1,0:T(8,128)(2,1)} %all-gather.8.cloned.1.call-done, bf16[512,1024]{1,0:T(8,128)(2,1)} %all-gather.4.cloned.1.call-done, bf16[1024,1024]{1,0:T(8,128)(2,1)} %all-gather.6.cloned.1.call-done), kind=kOutput, calls=%fused_computation.1 | convolution fusion | flops 2149580800 | bytes 6291456 | tf_op jit(solution)/shard_map/dot_general | solution.py:43
  128.1 0.0 copy-start.1
  128.1 0.0 copy-start.2
  128.1 0.0 reduce-scatter.2.cloned.1.call-update
  128.1 23.2 %reduce-scatter.2.cloned.1.call-done = bf16[128,1024]{1,0:T(8,128)(2,1)} async-done(((bf16[512,1024]{1,0:T(8,128)(2,1)}), bf16[128,1024]{1,0:T(8,128)(2,1)}) %reduce-scatter.2.cloned.1.call-update) | async-done | bytes 262160 | tf_op jit(solution)/shard_map/reduce_scatter | solution.py:17
  151.3 0.0 copy-done
  151.3 1.1 fusion
  152.4 1.2 multiply_reduce_fusion
  153.6 0.0 copy-done.1
  153.6 0.0 copy-done.2
  153.6 1.8 %add_convert_fusion = bf16[128,1024]{1,0:T(8,128)(2,1)} fusion(bf16[128,1024]{1,0:T(8,128)(2,1)} %reduce-scatter.2.cloned.1.call-done, bf16[128,1024]{1,0:T(8,128)(2,1)S(1)} %copy-done, f32[1024]{0:T(1024)S(1)} %copy-done.1, f32[1024]{0:T(1024)S(1)} %copy-done.2, f32[128]{0:T(128)S(1)} %add_rsqrt_fusion, f32[128]{0:T(128)S(1)} %broadcast_multiply_fusion), kind=kLoop, calls=%fused_computation.2 | loop fusion | flops 1179648 | bytes 795648 | tf_op jit(solution)/shard_map/convert_element_type | solution.py:47
  (2 shorter events, 0.0 us)
Async XLA Ops:
  6.5 21.8 %all-gather.4.cloned.1.call-start = ((), (), s32[]{:S(2)}) async-start(), calls=%async_computation.1 | async-start | bytes 1310720 | tf_op jit(solution)/shard_map/all_gather | solution.py:11
  7.3 68.3 %all-gather.6.cloned.1.call-start = ((), (), s32[]{:S(2)}) async-start(), calls=%async_computation.2 | async-start | bytes 2621440 | tf_op jit(solution)/shard_map/all_gather | solution.py:32
  8.0 114.3 %all-gather.8.cloned.1.call-start = ((), (), s32[]{:S(2)}) async-start(), calls=%async_computation.3 | async-start | bytes 2621440 | tf_op jit(solution)/shard_map/all_gather | solution.py:38
  8.7 142.6 %copy-start = (bf16[128,1024]{1,0:T(8,128)(2,1)S(1)}, bf16[128,1024]{1,0:T(8,128)(2,1)}, u32[]{:S(2)}) copy-start(bf16[128,1024]{1,0:T(8,128)(2,1)} %param.5) | copy-start | bytes 786436
  8.8 142.6 %reduce-scatter.2.cloned.1.call-start = ((), (), s32[]{:S(2)}) async-start(), calls=%async_computation.4 | async-start | bytes 1310720 | tf_op jit(solution)/shard_map/reduce_scatter | solution.py:17
  128.1 25.5 %copy-start.1 = (f32[1024]{0:T(1024)S(1)}, f32[1024]{0:T(1024)}, u32[]{:S(2)}) copy-start(f32[1024]{0:T(1024)} %param.9) | copy-start | bytes 12292
  128.1 25.5 %copy-start.2 = (f32[1024]{0:T(1024)S(1)}, f32[1024]{0:T(1024)}, u32[]{:S(2)}) copy-start(f32[1024]{0:T(1024)} %param.8) | copy-start | bytes 12292
Sparse Core Ops, SparseCore 0:
  8.9 19.4 all-gather.3
  29.9 45.6 all-gather.5
  77.2 45.0 all-gather.7
  128.3 22.9 reduce-scatter.1
where the time goes:
time: 162 us
  waiting for transfers between devices  139 us (86%)
  between operations  13.2 us (8%)
  matrix products  5.85 us (4%)
  other arithmetic  4.1 us (3%)
    all_gather x1, waiting for transfers between devices, shards(): up_block = lax.all_gather(w_up, 'fs', axis=0, tiled=True)  47.3 us
    all_gather x1, waiting for transfers between devices, shards(): down_block = lax.all_gather(w_down, 'fs', axis=1, tiled=True)  46.7 us
    reduce_scatter x1, waiting for transfers between devices, summed_rows(): lax.psum_scatter(whole, axis, scatter_dimension=0, tiled=True)  23.2 us
    all_gather x1, waiting for transfers between devices, over_all(): everything = lax.all_gather(share, axis, axis=dim, tiled=True)  19.6 us
    dot_general x1, matrix products, project(): return jnp.dot(picked, down_block, preferred_element_type=jnp.float32)  5.85 us
  transfers between devices with their start and end apart: 4, of which 4 were waited for; matrix products, arithmetic and copies ran while one was open for 0% of the time, Pallas kernels for 0%

commit v1 on v0

--- a/solution.py
+++ b/solution.py
@@ -35,7 +35,12 @@
         return squared_relu(jnp.dot(block_rows, up_block, preferred_element_type=jnp.float32))
 
     hidden = over_all(tokens, "tp", 0, activate)
-    down_block = lax.all_gather(w_down, "fs", axis=1, tiled=True)
+    ring = [w_down]
+    for hop in range(3):
+        ring.append(lax.ppermute(ring[-1], "fs", [(dev, (dev + 1) % 4) for dev in range(4)]))
+    down_block = jnp.roll(
+        jnp.concatenate(ring[::-1], axis=1), (lax.axis_index("fs") + 1) * ring[0].shape[1], axis=1
+    )
     own_count = tokens.shape[0]
 
     def project(offset, how_many):

time: 162 us -> 127 us (0.78)
  waiting for transfers between devices: 139 us -> 93.8 us
  local copies, waits for them, and re-layouts: 0.01 us -> 6.99 us
  starting transfers between devices: 0.12 us -> 3.19 us
    ppermute x0 -> x3, waiting for transfers between devices: none -> 56 us  [shards(): lax.ppermute(ring[-1], 'fs', [(dev, (dev + 1) % 4) for dev in range(4)])]
    all_gather x1 -> x0, waiting for transfers between devices: 46.7 us -> none  [shards(): down_block = lax.all_gather(w_down, 'fs', axis=1, tiled=True)]
    all_gather x1, waiting for transfers between devices: 47.3 us -> 12.7 us  [shards(): up_block = lax.all_gather(w_up, 'fs', axis=0, tiled=True)]
    all_gather x1, waiting for transfers between devices: 19.6 us -> 0.01 us  [over_all(): everything = lax.all_gather(share, axis, axis=dim, tiled=True)]
    unnamed x6 -> x15, local copies, waits for them, and re-layouts: 0.01 us -> 6.13 us
    ppermute x0 -> x3, starting transfers between devices: none -> 3.11 us  [shards(): lax.ppermute(ring[-1], 'fs', [(dev, (dev + 1) % 4) for dev in range(4)])]
  transfers between devices with their start and end apart: 4 -> 6, of which waited for: 4 -> 5; matrix products, arithmetic and copies ran while one was open for 0% -> 5% of each run, Pallas kernels for 0% -> 0%
where the time goes in v1:
time: 127 us
  waiting for transfers between devices  93.8 us (74%)
  between operations  13.1 us (10%)
  local copies, waits for them, and re-layouts  6.99 us (6%)
  matrix products  5.88 us (5%)
  other arithmetic  4.1 us (3%)
  starting transfers between devices  3.19 us (3%)
    ppermute x3, waiting for transfers between devices, shards(): lax.ppermute(ring[-1], 'fs', [(dev, (dev + 1) % 4) for dev in range(4)])  56 us
    reduce_scatter x1, waiting for transfers between devices, summed_rows(): lax.psum_scatter(whole, axis, scatter_dimension=0, tiled=True)  23.7 us
    all_gather x1, waiting for transfers between devices, shards(): up_block = lax.all_gather(w_up, 'fs', axis=0, tiled=True)  12.7 us
    unnamed x15, local copies, waits for them, and re-layouts  6.13 us
    dot_general x1, matrix products, project(): return jnp.dot(picked, down_block, preferred_element_type=jnp.float32)  5.88 us
    ppermute x3, starting transfers between devices, shards(): lax.ppermute(ring[-1], 'fs', [(dev, (dev + 1) % 4) for dev in range(4)])  3.11 us
  transfers between devices with their start and end apart: 6, of which 5 were waited for; matrix products, arithmetic and copies ran while one was open for 5% of the time, Pallas kernels for 0%

profile of v1, /device:TPU:0, one launch (start us, length us, event | category | flops | bytes accessed | tf_op | source)
XLA Modules:
  0.0 127.1 jit_solution(2147206913888353451)
XLA Ops:
  6.5 0.0 copy-start.1
  6.5 0.0 all-gather.3.cloned.1.call-start
  6.5 0.7 all-gather.3.cloned.1.call-update
  7.3 0.0 all-gather.5.cloned.1.call-start
  7.3 0.7 all-gather.5.cloned.1.call-update
  8.0 0.0 reduce-scatter.2.cloned.1.call-start
  8.1 3.1 %collective-permute-start = (bf16[1024,256]{1,0:T(8,128)(2,1)}, bf16[1024,256]{1,0:T(8,128)(2,1)S(1)}, u32[]{:S(2)}, u32[]{:S(2)}) collective-permute-start(bf16[1024,256]{1,0:T(8,128)(2,1)} %param.7), channel_id=1, source_target_pairs={{0,4},{4,8},{8,12},{12,0},{1,5},{5,9},{9,13},{13,1},{2,6},{6,10},{... | collective-permute-start | bytes 1572872 | tf_op jit(solution)/shard_map/ppermute | solution.py:40
  11.2 14.2 %collective-permute-done = bf16[1024,256]{1,0:T(8,128)(2,1)S(1)} collective-permute-done((bf16[1024,256]{1,0:T(8,128)(2,1)}, bf16[1024,256]{1,0:T(8,128)(2,1)S(1)}, u32[]{:S(2)}, u32[]{:S(2)}) %collective-permute-start) | collective-permute-done | bytes 524320 | tf_op jit(solution)/shard_map/ppermute | solution.py:40
  25.3 0.0 collective-permute-start.1
  25.3 14.9 %collective-permute-done.1 = bf16[1024,256]{1,0:T(8,128)(2,1)S(1)} collective-permute-done((bf16[1024,256]{1,0:T(8,128)(2,1)S(1)}, bf16[1024,256]{1,0:T(8,128)(2,1)S(1)}, u32[]{:S(2)}, u32[]{:S(2)}) %collective-permute-start.1) | collective-permute-done | bytes 524320 | tf_op jit(solution)/shard_map/ppermute | solution.py:40
  40.2 0.0 collective-permute-start.2
  40.2 26.9 %collective-permute-done.2 = bf16[1024,256]{1,0:T(8,128)(2,1)S(1)} collective-permute-done((bf16[1024,256]{1,0:T(8,128)(2,1)S(1)}, bf16[1024,256]{1,0:T(8,128)(2,1)S(1)}, u32[]{:S(2)}, u32[]{:S(2)}) %collective-permute-start.2) | collective-permute-done | bytes 524320 | tf_op jit(solution)/shard_map/ppermute | solution.py:40
  67.1 0.9 constant_dynamic-update-slice_fusion.7
  68.1 0.9 constant_dynamic-update-slice_fusion.6
  68.9 0.9 constant_dynamic-update-slice_fusion.5
  69.8 0.0 copy-done.1
  69.8 0.9 constant_dynamic-update-slice_fusion.4
  70.7 0.9 constant_dynamic-update-slice_fusion.3
  71.5 0.9 constant_dynamic-update-slice_fusion.2
  72.4 0.9 constant_dynamic-update-slice_fusion.1
  73.3 0.9 constant_dynamic-update-slice_fusion
  74.1 0.0 copy-start
  74.1 0.0 copy-start.2
  74.1 0.0 copy-start.3
  74.1 0.0 all-gather.3.cloned.1.call-done
  74.1 12.7 %all-gather.5.cloned.1.call-done = bf16[1024,1024]{1,0:T(8,128)(2,1)} async-done(((bf16[256,1024]{1,0:T(8,128)(2,1)}), bf16[1024,1024]{1,0:T(8,128)(2,1)}) %all-gather.5.cloned.1.call-update) | async-done | bytes 2097168 | tf_op jit(solution)/shard_map/all_gather | solution.py:32
  86.8 5.9 %fusion.2 = bf16[512,1024]{1,0:T(8,128)(2,1)} fusion(bf16[1024,2048]{1,0:T(8,128)(2,1)} %constant_dynamic-update-slice_fusion, s32[]{:T(128)S(6)} %select_n.14, bf16[512,1024]{1,0:T(8,128)(2,1)} %all-gather.3.cloned.1.call-done, bf16[1024,1024]{1,0:T(8,128)(2,1)} %all-gather.5.cloned.1.call-done), kind=kOutput, calls=%fused_computation.3 | convolution fusion | flops 2149580800 | bytes 6291460 | tf_op jit(solution)/shard_map/dot_general | solution.py:48
  92.7 0.0 reduce-scatter.2.cloned.1.call-update
  92.7 23.7 %reduce-scatter.2.cloned.1.call-done = bf16[128,1024]{1,0:T(8,128)(2,1)} async-done(((bf16[512,1024]{1,0:T(8,128)(2,1)}), bf16[128,1024]{1,0:T(8,128)(2,1)}) %reduce-scatter.2.cloned.1.call-update) | async-done | bytes 262160 | tf_op jit(solution)/shard_map/reduce_scatter | solution.py:17
  116.5 0.0 copy-done
  116.5 1.1 fusion.5
  117.6 1.2 multiply_reduce_fusion
  118.8 0.0 copy-done.2
  118.8 0.0 copy-done.3
  118.8 1.8 %add_convert_fusion = bf16[128,1024]{1,0:T(8,128)(2,1)} fusion(bf16[128,1024]{1,0:T(8,128)(2,1)} %reduce-scatter.2.cloned.1.call-done, bf16[128,1024]{1,0:T(8,128)(2,1)S(1)} %copy-done, f32[1024]{0:T(1024)S(1)} %copy-done.2, f32[1024]{0:T(1024)S(1)} %copy-done.3, f32[128]{0:T(128)S(1)} %add_rsqrt_fusion, f32[128]{0:T(128)S(1)} %broadcast_multiply_fusion), kind=kLoop, calls=%fused_computation.4 | loop fusion | flops 1179648 | bytes 795648 | tf_op jit(solution)/shard_map/convert_element_type | solution.py:52
  (2 shorter events, 0.0 us)
Async XLA Ops:
  6.5 63.3 %copy-start.1 = (bf16[1024,256]{1,0:T(8,128)(2,1)S(1)}, bf16[1024,256]{1,0:T(8,128)(2,1)}, u32[]{:S(2)}) copy-start(bf16[1024,256]{1,0:T(8,128)(2,1)} %param.7) | copy-start | bytes 1572868
  6.5 67.6 %all-gather.3.cloned.1.call-start = ((), (), s32[]{:S(2)}) async-start(), calls=%async_computation.1 | async-start | bytes 1310720 | tf_op jit(solution)/shard_map/all_gather | solution.py:11
  7.3 79.6 %all-gather.5.cloned.1.call-start = ((), (), s32[]{:S(2)}) async-start(), calls=%async_computation.2 | async-start | bytes 2621440 | tf_op jit(solution)/shard_map/all_gather | solution.py:32
  8.0 108.5 %reduce-scatter.2.cloned.1.call-start = ((), (), s32[]{:S(2)}) async-start(), calls=%async_computation.3 | async-start | bytes 1310720 | tf_op jit(solution)/shard_map/reduce_scatter | solution.py:17
  8.1 17.3 %collective-permute-start = (bf16[1024,256]{1,0:T(8,128)(2,1)}, bf16[1024,256]{1,0:T(8,128)(2,1)S(1)}, u32[]{:S(2)}, u32[]{:S(2)}) collective-permute-start(bf16[1024,256]{1,0:T(8,128)(2,1)} %param.7), channel_id=1, source_target_pairs={{0,4},{4,8},{8,12},{12,0},{1,5},{5,9},{9,13},{13,1},{2,6},{6,10},{... | collective-permute-start | bytes 1572872 | tf_op jit(solution)/shard_map/ppermute | solution.py:40
  25.3 14.9 %collective-permute-start.1 = (bf16[1024,256]{1,0:T(8,128)(2,1)S(1)}, bf16[1024,256]{1,0:T(8,128)(2,1)S(1)}, u32[]{:S(2)}, u32[]{:S(2)}) collective-permute-start(bf16[1024,256]{1,0:T(8,128)(2,1)S(1)} %collective-permute-done), channel_id=1, source_target_pairs={{0,4},{4,8},{8,12},{12,0},{1,5},{5,9},{9,13},{13,1},{2,6},{6,10},{... | collective-permute-start | bytes 1572872 | tf_op jit(solution)/shard_map/ppermute | solution.py:40
  40.2 26.9 %collective-permute-start.2 = (bf16[1024,256]{1,0:T(8,128)(2,1)S(1)}, bf16[1024,256]{1,0:T(8,128)(2,1)S(1)}, u32[]{:S(2)}, u32[]{:S(2)}) collective-permute-start(bf16[1024,256]{1,0:T(8,128)(2,1)S(1)} %collective-permute-done.1), channel_id=1, source_target_pairs={{0,4},{4,8},{8,12},{12,0},{1,5},{5,9},{9,13},{13,1},{2,6},{6,10},{... | collective-permute-start | bytes 1572872 | tf_op jit(solution)/shard_map/ppermute | solution.py:40
  74.1 42.4 %copy-start = (bf16[128,1024]{1,0:T(8,128)(2,1)S(1)}, bf16[128,1024]{1,0:T(8,128)(2,1)}, u32[]{:S(2)}) copy-start(bf16[128,1024]{1,0:T(8,128)(2,1)} %param.5) | copy-start | bytes 786436
  74.1 44.6 %copy-start.2 = (f32[1024]{0:T(1024)S(1)}, f32[1024]{0:T(1024)}, u32[]{:S(2)}) copy-start(f32[1024]{0:T(1024)} %param.9) | copy-start | bytes 12292
  74.1 44.7 %copy-start.3 = (f32[1024]{0:T(1024)S(1)}, f32[1024]{0:T(1024)}, u32[]{:S(2)}) copy-start(f32[1024]{0:T(1024)} %param.8) | copy-start | bytes 12292
Sparse Core Ops, SparseCore 0:
  8.9 19.4 all-gather.2
  29.9 56.8 all-gather.4
  92.9 23.5 reduce-scatter.1
